TPU v7x, 32 devices: a whole 2x2x4 slice. The times are simulated.
32 devices in a mesh: fs: 4 (over y, x), tp: 8 (over z, core).
Axes of the slice: x: 2, y: 2, z: 4, core: 2. Of those that a mesh axis runs over, the one named last changes fastest.
Arguments:
- prompt: bfloat16 [4096, 2048], P(('fs', 'tp')), may hold values from -6 to 6
- norm_gain: float32 [2048], P('tp'), may hold values from 0.1 to 1.9
- gate_master: float32 [8, 2, 512, 2048], P(None, None, 'fs', 'tp'), may hold values from -0.125 to 0.125
- up_master: float32 [8, 2, 512, 2048], P(None, None, 'fs', 'tp'), may hold values from -0.125 to 0.125
- down_master: float32 [8, 2, 512, 2048], P(None, None, 'fs', 'tp'), may hold values from -0.25 to 0.25
- group_pick: int32 [4096, 1], P(('fs', 'tp')), may hold values from 0 to 7; in each aligned block of 128 rows (0 to 127, 128 to 255, ...) at most 32 rows name the same one
- route_weight: bfloat16 [4096, 2], P(('fs', 'tp')), may hold values from 0.099609375 to 1
Outputs:
- gate_serve: bfloat16 [8, 2, 512, 2048], P('tp', None, 'fs')
- up_serve: bfloat16 [8, 2, 512, 2048], P('tp', None, 'fs')
- down_serve: bfloat16 [8, 2, 512, 2048], P('tp', None, 'fs')
- mixed: bfloat16 [4096, 2048], P(('fs', 'tp'))
Inputs may be any that keep to these rules, and one draw needn't show every extreme that they name: `group_pick`: in the rows of one device no group is named by more than 32 rows, and in every draw some device's rows name one group exactly 32 times.
All inputs are finite; a program needn't handle non-finite values.
Results may differ from a plain program's by a relative error of at most 0.0081.
Values may be sent and summed in bfloat16 or wider, within the bound.
A program may use at most 64 MiB of HBM per device.

v0:
```python
import functools

import jax
import jax.numpy as jnp
from jax import lax
from jax.experimental import pallas as pl
from jax.experimental.pallas import tpu as pltpu
from jax.sharding import PartitionSpec as P

EPS = 1e-06
MESH = pl.DeviceIdType.MESH
LANES = 128


def expert_rows(group_rows, weights, pieces):
    gate_piece, up_piece, down_piece = pieces
    expert_count = gate_piece.shape[1]
    unit_count = gate_piece.shape[2]
    model_width = gate_piece.shape[3]
    row_count = group_rows.shape[0]
    gate_matrix = gate_piece.reshape(expert_count * unit_count, model_width)
    up_matrix = up_piece.reshape(expert_count * unit_count, model_width)
    down_matrix = down_piece.reshape(expert_count * unit_count, model_width)
    gate_pre = jnp.einsum("sd,hd->sh", group_rows, gate_matrix, preferred_element_type=jnp.float32)
    up_pre = jnp.einsum("sd,hd->sh", group_rows, up_matrix, preferred_element_type=jnp.float32)
    active = (jax.nn.silu(gate_pre) * up_pre).reshape(row_count, expert_count, unit_count)
    hidden = (weights.astype(jnp.float32)[:, :, None] * active).reshape(
        row_count, expert_count * unit_count
    )
    hidden = hidden.astype(jnp.bfloat16)
    return jnp.dot(hidden, down_matrix, preferred_element_type=jnp.float32)


def flipped(index, mask, size):
    total, bit = 0, 1
    while bit < size:
        digit = lax.rem(lax.div(index, bit), 2)
        total = total + bit * ((1 - digit) if mask & bit else digit)
        bit *= 2
    return total


def exchange_kernel(
    dims,
    gate_in, up_in, down_in, rows_in, placing_ref,
    gate_out, up_out, down_out, mixed_ref,
    xrows, hidden, psend, racc, qsend, qacc, rsum, ret,
    rows_s, rows_r, w_s, w_r, fwd_s, fwd_r, red_s, red_r, sec_s, sec_r, ret_s, ret_r, loc,
):
    fs_n, tp_n, experts, units, width, model, cap = dims
    f = lax.axis_index("fs")
    t = lax.axis_index("tp")
    tp_peer = [flipped(t, k, tp_n) for k in range(tp_n)]
    fs_peer = [flipped(f, j, fs_n) for j in range(fs_n)]

    barrier = pltpu.get_barrier_semaphore()
    for k in range(1, tp_n):
        pl.semaphore_signal(barrier, inc=1, device_id=(f, tp_peer[k]), device_id_type=MESH)
    for j in range(1, fs_n):
        pl.semaphore_signal(barrier, inc=1, device_id=(fs_peer[j], t), device_id_type=MESH)
    pl.semaphore_wait(barrier, tp_n - 1 + fs_n - 1)

    def columns(index):
        return pl.ds(pl.multiple_of(index * width, width), width)

    def remote(src, dst, send, recv, fs_to, tp_to):
        return pltpu.make_async_remote_copy(
            src_ref=src, dst_ref=dst, send_sem=send, recv_sem=recv,
            device_id=(fs_to, tp_to), device_id_type=MESH,
        )

    far_first = [1] + list(range(tp_n - 1, 1, -1))
    pieces = [0] + far_first
    own_rows = pltpu.make_async_copy(rows_in.at[t], xrows.at[f, t], loc.at[0])
    own_rows.start()
    rows_copy = {}
    for k in far_first:
        rows_copy[k] = remote(
            rows_in.at[tp_peer[k]], xrows.at[f, t], rows_s.at[k], rows_r.at[k], f, tp_peer[k]
        )
        rows_copy[k].start()
    w_copy, own_w = {}, []
    for m, (src, dst) in enumerate(((gate_in, gate_out), (up_in, up_out), (down_in, down_out))):
        own = pltpu.make_async_copy(src.at[t], dst.at[:, columns(t)], loc.at[1 + m])
        own.start()
        own_w.append(own)
        for k in far_first:
            w_copy[m, k] = remote(
                src.at[tp_peer[k]], dst.at[:, columns(t)], w_s.at[m, k], w_r.at[m, k], f, tp_peer[k]
            )

    fwd_copy = {}
    for k in pieces:
        if k == 0:
            own_rows.wait()
        else:
            rows_copy[k].wait_send()
            w_copy[0, k].start()
            rows_copy[k].wait_recv()
        for j in range(fs_n - 1, 0, -1):
            fwd_copy[k, j] = remote(
                xrows.at[f, tp_peer[k]], xrows.at[f, tp_peer[k]],
                fwd_s.at[k, j], fwd_r.at[k, j], fs_peer[j], t,
            )
            fwd_copy[k, j].start()
    for m in (1, 2):
        for k in far_first:
            w_copy[m - 1, k].wait_send()
            w_copy[m, k].start()
    for copy in fwd_copy.values():
        copy.wait_recv()
    for m in range(2):
        own_w[m].wait()
        for k in range(1, tp_n):
            w_copy[m, k].wait_recv()

    block = tp_n * cap

    @pl.loop(0, fs_n)
    def _(b):
        tile = xrows[b].reshape(block, model + LANES)
        x = tile[:, :model]
        route = tile[:, model:].astype(jnp.float32)
        nt = (((1,), (1,)), ((), ()))
        gate = lax.dot_general(x, gate_out[...], nt, preferred_element_type=jnp.float32)
        up = lax.dot_general(x, up_out[...], nt, preferred_element_type=jnp.float32)
        active = gate / (1.0 + jnp.exp(-gate)) * up
        for e in range(experts):
            at = slice(e * units, (e + 1) * units)
            hidden[b, :, at] = (route[:, e : e + 1] * active[:, at]).astype(jnp.bfloat16)

    first_copy, second_copy, ret_copy = {}, {}, {}
    half = width // 2
    order = ((1, 2), (2, 1))

    def partial(index, k, h):
        at = pl.ds(pl.multiple_of(tp_peer[k] * width + h * half, half), half)
        return jnp.dot(hidden[index], down_out[:, at], preferred_element_type=jnp.float32)

    def first_step(k):
        for h, (a, b) in enumerate(order):
            for n, index in enumerate((fs_peer[a], fs_peer[a ^ b])):
                psend[k, h, n] = partial(index, k, h).astype(jnp.bfloat16)
        for h, (a, b) in enumerate(order):
            first_copy[k, h] = remote(
                psend.at[k, h], racc.at[k, h], red_s.at[k, h], red_r.at[k, h], fs_peer[a], t
            )
            first_copy[k, h].start()

    def second_step(k):
        for h, (a, b) in enumerate(order):
            part = partial(fs_peer[b], k, h)
            first_copy[k, h].wait_recv()
            qsend[k, h] = (part + racc[k, h, 1].astype(jnp.float32)).astype(jnp.bfloat16)
        for h, (a, b) in enumerate(order):
            second_copy[k, h] = remote(
                qsend.at[k, h], qacc.at[k, h], sec_s.at[k, h], sec_r.at[k, h], fs_peer[b], t
            )
            second_copy[k, h].start()

    def reduce_and_return(k):
        col = columns(tp_peer[k])
        for h in range(2):
            total = partial(f, k, h) + racc[k, h, 0].astype(jnp.float32)
            second_copy[k, h].wait_recv()
            total = total + qacc[k, h].astype(jnp.float32)
            rsum[k, :, :, h * half : (h + 1) * half] = total.astype(jnp.bfloat16).reshape(
                tp_n, cap, half
            )
        for kk in far_first:
            ret_copy[k, kk] = remote(
                rsum.at[k, tp_peer[kk]], ret.at[t, :, col],
                ret_s.at[k, kk], ret_r.at[k, kk], f, tp_peer[kk],
            )
            ret_copy[k, kk].start()
        ret[t, :, col] = rsum[k, t]

    for step in range(tp_n + 2):
        if step < tp_n:
            k = pieces[step]
            if k == 0:
                own_w[2].wait()
            else:
                w_copy[2, k].wait_recv()
            first_step(k)
        if 1 <= step <= tp_n:
            second_step(pieces[step - 1])
        if step >= 2:
            reduce_and_return(pieces[step - 2])

    for copy in ret_copy.values():
        copy.wait_recv()
    mixed_ref[...] = lax.dot_general(
        placing_ref[...], ret[...].reshape(block, model), (((0,), (0,)), ((), ())),
        preferred_element_type=jnp.float32,
    ).astype(jnp.bfloat16)

    for k in far_first:
        w_copy[2, k].wait_send()
    for group in (fwd_copy, first_copy, second_copy, ret_copy):
        for copy in group.values():
            copy.wait_send()


def fused_device(fs_n, gate_local, up_local, down_local, normed, placing, route_weight, capacity):
    tp_n, experts, units, width = gate_local.shape
    tokens, model = normed.shape
    packed = jnp.concatenate(
        [normed, jnp.pad(route_weight, ((0, 0), (0, LANES - route_weight.shape[1])))], axis=1
    )
    rows = jnp.dot(placing, packed, preferred_element_type=jnp.float32).astype(jnp.bfloat16)
    rows = rows.reshape(tp_n, capacity, model + LANES)
    flat = experts * units
    block = tp_n * capacity
    bf16 = jnp.bfloat16
    dma = pltpu.SemaphoreType.DMA
    served = jax.ShapeDtypeStruct((flat, model), bf16)
    vmem = pl.BlockSpec(memory_space=pltpu.VMEM)
    hbm = pl.BlockSpec(memory_space=pl.ANY)
    dims = (fs_n, tp_n, experts, units, width, model, capacity)
    gate_serve, up_serve, down_serve, mixed = pl.pallas_call(
        functools.partial(exchange_kernel, dims),
        out_shape=(served, served, served, jax.ShapeDtypeStruct((tokens, model), bf16)),
        in_specs=[hbm, hbm, hbm, hbm, vmem],
        out_specs=(vmem, vmem, vmem, vmem),
        scratch_shapes=[
            pltpu.VMEM((fs_n, tp_n, capacity, model + LANES), bf16),
            pltpu.VMEM((fs_n, block, flat), bf16),
            pltpu.VMEM((tp_n, 2, 2, block, width // 2), bf16),
            pltpu.VMEM((tp_n, 2, 2, block, width // 2), bf16),
            pltpu.VMEM((tp_n, 2, block, width // 2), bf16),
            pltpu.VMEM((tp_n, 2, block, width // 2), bf16),
            pltpu.VMEM((tp_n, tp_n, capacity, width), bf16),
            pltpu.VMEM((tp_n, capacity, model), bf16),
            dma((tp_n,)), dma((tp_n,)),
            dma((3, tp_n)), dma((3, tp_n)),
            dma((tp_n, fs_n)), dma((tp_n, fs_n)),
            dma((tp_n, 2)), dma((tp_n, 2)),
            dma((tp_n, 2)), dma((tp_n, 2)),
            dma((tp_n, tp_n)), dma((tp_n, tp_n)),
            dma((4,)),
        ],
        compiler_params=pltpu.CompilerParams(collective_id=0, has_side_effects=True),
    )(
        gate_local.reshape(tp_n, flat, width),
        up_local.reshape(tp_n, flat, width),
        down_local.reshape(tp_n, flat, width),
        rows,
        placing,
    )
    shape = (1, experts, units, model)
    return gate_serve.reshape(shape), up_serve.reshape(shape), down_serve.reshape(shape), mixed


def per_device(prompt, norm_gain, gate_master, up_master, down_master, group_pick, route_weight):
    group_total = lax.axis_size("tp")
    fs_n = lax.axis_size("fs")
    gate_local = (gate_master * norm_gain).astype(jnp.bfloat16)
    up_local = (up_master * norm_gain).astype(jnp.bfloat16)
    down_local = down_master.astype(jnp.bfloat16)
    values = prompt.astype(jnp.float32)
    normed = (values * lax.rsqrt(jnp.mean(values * values, axis=1, keepdims=True) + EPS)).astype(
        jnp.bfloat16
    )
    tok_count = prompt.shape[0]
    capacity = 2 * tok_count // group_total
    slot_total = group_total * capacity
    chosen = group_pick[:, 0]
    member = (chosen[:, None] == jnp.arange(group_total, dtype=jnp.int32)[None, :]).astype(
        jnp.int32
    )
    slot_rank = jnp.sum(jnp.cumsum(member, axis=0) * member, axis=1) - 1
    target = chosen * capacity + slot_rank
    placing = (jnp.arange(slot_total, dtype=jnp.int32)[:, None] == target[None, :]).astype(
        jnp.bfloat16
    )
    width, units = gate_master.shape[3], gate_master.shape[2]
    small = group_total in (4, 8) and fs_n == 4
    if small and width % (2 * LANES) == 0 and units % LANES == 0 and capacity % 16 == 0:
        return fused_device(
            fs_n, gate_local, up_local, down_local, normed, placing, route_weight, capacity
        )
    gate_serve, up_serve, down_serve = (
        lax.all_to_all(gate_local, "tp", split_axis=0, concat_axis=3, tiled=True),
        lax.all_to_all(up_local, "tp", split_axis=0, concat_axis=3, tiled=True),
        lax.all_to_all(down_local, "tp", split_axis=0, concat_axis=3, tiled=True),
    )
    send_rows = jnp.dot(placing, normed, preferred_element_type=jnp.float32).astype(jnp.bfloat16)
    send_weights = jnp.dot(placing, route_weight, preferred_element_type=jnp.float32).astype(
        jnp.bfloat16
    )
    got_rows, got_weights = (
        lax.all_to_all(
            send_rows.reshape(group_total, capacity, -1),
            "tp",
            split_axis=0,
            concat_axis=0,
            tiled=True,
        ),
        lax.all_to_all(
            send_weights.reshape(group_total, capacity, -1),
            "tp",
            split_axis=0,
            concat_axis=0,
            tiled=True,
        ),
    )
    group_rows = got_rows.reshape(slot_total, -1)
    weights = got_weights.reshape(slot_total, -1)
    gathered = (
        lax.all_gather(gate_serve, "fs", axis=2, tiled=True),
        lax.all_gather(up_serve, "fs", axis=2, tiled=True),
        lax.all_gather(down_serve, "fs", axis=2, tiled=True),
    )
    summed = expert_rows(group_rows, weights, gathered)
    result = summed.astype(jnp.bfloat16).reshape(group_total, capacity, -1)
    returned = lax.all_to_all(result, "tp", split_axis=0, concat_axis=0, tiled=True)
    mixed = jnp.einsum(
        "st,sd->td", placing, returned.reshape(slot_total, -1), preferred_element_type=jnp.float32
    ).astype(jnp.bfloat16)
    return (gate_serve, up_serve, down_serve, mixed)


def solution(mesh):
    placed = (
        P(("fs", "tp"), None),
        P("tp"),
        P(None, None, "fs", "tp"),
        P(None, None, "fs", "tp"),
        P(None, None, "fs", "tp"),
        P(("fs", "tp"), None),
        P(("fs", "tp"), None),
    )
    return jax.shard_map(
        per_device,
        mesh=mesh,
        in_specs=placed,
        out_specs=(
            P("tp", None, "fs", None),
            P("tp", None, "fs", None),
            P("tp", None, "fs", None),
            P(("fs", "tp"), None),
        ),
        check_vma=False,
    )
```

profile of v0, /device:TPU:0, one launch (start us, length us, event | category | flops | bytes accessed | tf_op | source)
XLA Modules:
  0.0 156.1 jit_solution(10845844866042131391)
XLA Ops:
  0.6 0.0 copy-start
  0.6 1.4 fusion.1
  2.0 0.8 copy.12
  2.8 0.7 fusion.11
  3.6 0.2 reduce_window_sum.11
  3.7 0.8 select_reduce_fusion
  4.6 0.7 add_add_fusion
  5.2 0.7 fusion.9.placing_ref
  5.9 1.2 fusion.2
  7.1 0.0 copy-start.1
  7.1 0.0 copy-start.2
  7.1 0.0 copy-start.6
  7.1 1.4 convolution_convert_fusion
  8.5 0.0 copy-done
  8.6 1.1 convert_element_type.28
  9.6 0.0 copy-done.1
  9.7 0.2 copy-done.2
  9.9 0.0 copy-done.6
  9.9 1.8 %multiply_convert_fusion = (bf16[8,2,128,256]{3,2,1,0:T(8,128)(2,1)}, bf16[8,2,128,256]{3,2,1,0:T(8,128)(2,1)}) fusion(f32[8,2,128,256]{3,2,1,0:T(8,128)S(1)} %copy-done.1, f32[256]{0:T(256)S(1)} %copy-done.6, f32[8,2,128,256]{3,2,1,0:T(8,128)S(1)} %copy-done.2), kind=kLoop, calls=%fused_computation.1 | loop fusion | flops 2097152 | bytes 6292480 | tf_op jit(solution)/shard_map/convert_element_type | solution.py:259
  11.7 139.2 %shard_map.102 = (bf16[256,2048]{1,0:T(8,128)(2,1)}, bf16[256,2048]{1,0:T(8,128)(2,1)}, bf16[256,2048]{1,0:T(8,128)(2,1)}, bf16[128,2048]{1,0:T(8,128)(2,1)}) custom-call(bf16[8,256,256]{2,1,0:T(8,128)(2,1)} %bitcast.11, bf16[8,256,256]{2,1,0:T(8,128)(2,1)} %bitcast.10, bf16[8,256,256]{2,1,0:T(8,128)(2,1)} %bitcast.9, bf16[8,32,2176]{2,1,0:T(8,128)(2,1)} %bitcast.12, ...), custom_call_target="tpu_custom_call" | custom-call | tf_op jit(solution)/shard_map/pallas_call | solution.py:221
  150.9 0.0 copy-start.4
  150.9 0.0 copy-start.3
  150.9 2.5 %copy.17 = bf16[1,2,128,2048]{3,2,1,0:T(8,128)(2,1)} copy(bf16[1,2,128,2048]{3,2,1,0:T(8,128)(2,1)} %bitcast.15) | data formatting | bytes 2097152
  153.3 0.0 copy-done.4
  153.3 0.0 copy-start.5
  153.3 1.0 copy.18
  154.3 0.0 copy-done.3
  154.3 1.0 copy.19
  155.3 0.0 copy-done.5
  155.3 0.8 copy.20
  (1 shorter events, 0.0 us)
Async XLA Ops:
  0.6 7.9 %copy-start = (f32[8,2,128,256]{3,2,1,0:T(8,128)S(1)}, f32[8,2,128,256]{3,2,1,0:T(8,128)}, u32[]{:S(2)}) copy-start(f32[8,2,128,256]{3,2,1,0:T(8,128)} %param.11) | copy-start | bytes 6291460
  7.1 2.6 %copy-start.1 = (f32[8,2,128,256]{3,2,1,0:T(8,128)S(1)}, f32[8,2,128,256]{3,2,1,0:T(8,128)}, u32[]{:S(2)}) copy-start(f32[8,2,128,256]{3,2,1,0:T(8,128)} %param.10) | copy-start | bytes 6291460
  7.1 2.8 %copy-start.2 = (f32[8,2,128,256]{3,2,1,0:T(8,128)S(1)}, f32[8,2,128,256]{3,2,1,0:T(8,128)}, u32[]{:S(2)}) copy-start(f32[8,2,128,256]{3,2,1,0:T(8,128)} %param.9) | copy-start | bytes 6291460
  7.1 2.8 %copy-start.6 = (f32[256]{0:T(256)S(1)}, f32[256]{0:T(256)}, u32[]{:S(2)}) copy-start(f32[256]{0:T(256)} %param.8) | copy-start | bytes 3076
  150.9 2.5 %copy-start.4 = (bf16[256,2048]{1,0:T(8,128)(2,1)S(1)}, bf16[256,2048]{1,0:T(8,128)(2,1)}, u32[]{:S(2)}) copy-start(bf16[256,2048]{1,0:T(8,128)(2,1)} %get-tuple-element.9) | copy-start | bytes 3145732
  150.9 3.4 %copy-start.3 = (bf16[256,2048]{1,0:T(8,128)(2,1)S(1)}, bf16[256,2048]{1,0:T(8,128)(2,1)}, u32[]{:S(2)}) copy-start(bf16[256,2048]{1,0:T(8,128)(2,1)} %get-tuple-element.10) | copy-start | bytes 3145732
  153.3 1.9 %copy-start.5 = (bf16[128,2048]{1,0:T(8,128)(2,1)S(1)}, bf16[128,2048]{1,0:T(8,128)(2,1)}, u32[]{:S(2)}) copy-start(bf16[128,2048]{1,0:T(8,128)(2,1)} %get-tuple-element.21) | copy-start | bytes 1572868
where the time goes:
time: 156 us
  Pallas kernels  139 us (89%)
  other arithmetic  8.54 us (5%)
  local copies, waits for them, and re-layouts  6.21 us (4%)
    pallas_call x1, Pallas kernels, fused_device(): pl.pallas_call(functools.partial(exchange_kernel, dims), out_shape=(serve...  139 us
    unnamed x19, local copies, waits for them, and re-layouts  6.21 us

commit v1 on v0

v1 whole, which is shorter than its diff:
```python
import functools

import jax
import jax.numpy as jnp
from jax import lax
from jax.experimental import pallas as pl
from jax.experimental.pallas import tpu as pltpu
from jax.sharding import PartitionSpec as P

EPS = 1e-06
MESH = pl.DeviceIdType.MESH
LANES = 128
NT = (((1,), (1,)), ((), ()))
TN = (((0,), (0,)), ((), ()))


def expert_rows(group_rows, weights, pieces):
    gate_piece, up_piece, down_piece = pieces
    expert_count = gate_piece.shape[1]
    unit_count = gate_piece.shape[2]
    model_width = gate_piece.shape[3]
    row_count = group_rows.shape[0]
    gate_matrix = gate_piece.reshape(expert_count * unit_count, model_width)
    up_matrix = up_piece.reshape(expert_count * unit_count, model_width)
    down_matrix = down_piece.reshape(expert_count * unit_count, model_width)
    gate_pre = jnp.einsum("sd,hd->sh", group_rows, gate_matrix, preferred_element_type=jnp.float32)
    up_pre = jnp.einsum("sd,hd->sh", group_rows, up_matrix, preferred_element_type=jnp.float32)
    active = (jax.nn.silu(gate_pre) * up_pre).reshape(row_count, expert_count, unit_count)
    hidden = (weights.astype(jnp.float32)[:, :, None] * active).reshape(
        row_count, expert_count * unit_count
    )
    hidden = hidden.astype(jnp.bfloat16)
    return jnp.dot(hidden, down_matrix, preferred_element_type=jnp.float32)


def flipped(index, mask, size):
    total, bit = 0, 1
    while bit < size:
        digit = lax.rem(lax.div(index, bit), 2)
        total = total + bit * ((1 - digit) if mask & bit else digit)
        bit *= 2
    return total


def exchange_kernel(
    dims,
    prompt_in, gain_in, gate_in, up_in, down_in, pick_in, route_in,
    gate_out, up_out, down_out, ret, placing_ref,
    gain_ref, pick_ref, route_ref, down_all, prompt, stage, wsend, rows, xrows, acc, hid, hcat, rsum, route_pad,
    load, rows_s, rows_r, w_s, w_r, fx_s, fx_r, dx_s, dx_r, h_s, h_r, ret_s, ret_r, loc,
):
    fs_n, tp_n, experts, units, width, model, cap = dims
    flat, block, tokens = experts * units, tp_n * cap, prompt.shape[0]
    f = lax.axis_index("fs")
    t = lax.axis_index("tp")
    tp_peer = [flipped(t, k, tp_n) for k in range(tp_n)]
    fs_peer = [flipped(f, j, fs_n) for j in range(fs_n)]

    near = list(range(2, tp_n)) + [1]
    late = [tp_n // 2, tp_n // 2 + 1]
    early = [k for k in near if k not in late]
    pairs = list(range(0, tp_n, 2))
    down_order = early + late

    prompt_load = pltpu.make_async_copy(prompt_in, prompt, load.at[3, 0])
    small_loads = [
        pltpu.make_async_copy(src, dst, load.at[3, 1 + i])
        for i, (src, dst) in enumerate(
            ((pick_in, pick_ref), (route_in, route_ref), (gain_in, gain_ref))
        )
    ]
    for copy in small_loads:
        copy.start()
    prompt_load.start()
    sources = (gate_in, up_in, down_in)
    loads = {}

    def load_weight(m, k):
        loads[m, k] = pltpu.make_async_copy(
            sources[m].at[tp_peer[k]], stage.at[m, k], load.at[m, k]
        )
        loads[m, k].start()

    for k in early:
        load_weight(2, k)
    for m in range(2):
        for k in near:
            load_weight(m, k)
    for k in late:
        load_weight(2, k)
    for m in range(3):
        load_weight(m, 0)

    barrier = pltpu.get_barrier_semaphore()
    for k in range(1, tp_n):
        pl.semaphore_signal(barrier, inc=1, device_id=(f, tp_peer[k]), device_id_type=MESH)
    for j in range(1, fs_n):
        pl.semaphore_signal(barrier, inc=1, device_id=(fs_peer[j], t), device_id_type=MESH)

    def columns(index):
        return pl.ds(pl.multiple_of(index * width, width), width)

    def remote(src, dst, send, recv, fs_to, tp_to):
        return pltpu.make_async_remote_copy(
            src_ref=src, dst_ref=dst, send_sem=send, recv_sem=recv,
            device_id=(fs_to, tp_to), device_id_type=MESH,
        )

    for copy in small_loads:
        copy.wait()
    pick = pick_ref[...].astype(jnp.float32)
    group_id = lax.broadcasted_iota(jnp.int32, (tp_n, tokens), 0).astype(jnp.float32)
    member = jnp.where(group_id == pick, 1.0, 0.0)
    ahead = jnp.where(
        lax.broadcasted_iota(jnp.int32, (tokens, tokens), 0)
        <= lax.broadcasted_iota(jnp.int32, (tokens, tokens), 1),
        1.0, 0.0,
    ).astype(jnp.bfloat16)
    count = jnp.dot(member.astype(jnp.bfloat16), ahead, preferred_element_type=jnp.float32)
    rank = jnp.sum(member * count, axis=0, keepdims=True) - 1.0
    target = pick * cap + rank
    slot = lax.broadcasted_iota(jnp.int32, (block, tokens), 0).astype(jnp.float32)
    placing = jnp.where(slot == target, 1.0, 0.0).astype(jnp.bfloat16)
    placing_ref[...] = placing
    route_pad[...] = jnp.zeros_like(route_pad)
    route_pad[0:experts, :] = route_ref[...]
    routed = lax.dot_general(placing, route_pad[...], NT, preferred_element_type=jnp.float32)
    rows[:, :, model:] = routed.astype(jnp.bfloat16).reshape(tp_n, cap, LANES)
    prompt_load.wait()
    values = prompt[...].astype(jnp.float32)
    scale = lax.rsqrt(jnp.mean(values * values, axis=1, keepdims=True) + EPS)
    normed = (values * scale).astype(jnp.bfloat16)
    rows[:, :, :model] = (
        jnp.dot(placing, normed, preferred_element_type=jnp.float32)
        .astype(jnp.bfloat16)
        .reshape(tp_n, cap, model)
    )

    pl.semaphore_wait(barrier, tp_n - 1 + fs_n - 1)

    rows_copy = {}
    for k in near:
        rows_copy[k] = remote(
            rows.at[tp_peer[k]], xrows.at[f, t], rows_s.at[k], rows_r.at[k], f, tp_peer[k]
        )
        rows_copy[k].start()
    own_rows = pltpu.make_async_copy(rows.at[t], xrows.at[f, t], loc.at[0])
    own_rows.start()

    own_down = pl.ds(pl.multiple_of(f * flat, flat), flat)

    def landing(m):
        if m == 2:
            return down_all.at[own_down, columns(t)]
        return (gate_out, up_out)[m].at[:, columns(t)]

    w_copy = {}

    def convert(m, k):
        loads[m, k].wait()
        value = stage[m, k]
        if m < 2:
            value = value * gain_ref[...]
        value = value.astype(jnp.bfloat16)
        if k > 0:
            wsend[m, k] = value
            w_copy[m, k] = remote(
                wsend.at[m, k], landing(m), w_s.at[m, k], w_r.at[m, k], f, tp_peer[k]
            )
        elif m == 2:
            down_all[own_down, columns(t)] = value
        else:
            (gate_out, up_out)[m][:, columns(t)] = value

    for k in early:
        convert(2, k)
    for k in early:
        w_copy[2, k].start()
    for k in near:
        convert(0, k)
    for k in late:
        w_copy[0, k].start()
    for m in range(3):
        convert(m, 0)

    def spread(copies, k, piece, send, recv):
        first, second = (1, 2) if (k // 2 + k) % 2 == 0 else (2, 1)
        origin = {0: f, 1: fs_peer[first], 2: fs_peer[second]}

        def go(slot, owner, to):
            ref = piece(owner)
            copies[k, slot] = remote(
                ref, ref, send.at[k, slot], recv.at[k, slot], fs_peer[to], t
            )
            copies[k, slot].start()

        def own():
            go(0, f, first)
            go(1, f, second)

        def relay():
            copies[k, 0].wait_recv()
            go(2, fs_peer[first], second)

        return own, relay

    fx, dx = {}, {}

    def rows_piece(k):
        return lambda owner: xrows.at[owner, tp_peer[k]]

    def down_piece(k):
        return lambda owner: down_all.at[
            pl.ds(pl.multiple_of(owner * flat, flat), flat), columns(tp_peer[k])
        ]

    pending = []

    def advance(relay, lag):
        pending.append(relay)
        while len(pending) > lag:
            pending.pop(0)()

    own_rows.wait()
    for k in [0, 1] + near[:-1]:
        if k > 0:
            rows_copy[k].wait_recv()
        own, relay = spread(fx, k, rows_piece(k), fx_s, fx_r)
        own()
        if k in early:
            rows_copy[k].wait_send()
            w_copy[0, k].start()
        if k > 0:
            convert(1, k)
        if k in late:
            rows_copy[k].wait_send()
            w_copy[1, k].start()
        advance(relay, 1)
    for k in late:
        convert(2, k)
    for k in [0, 1] + [k for k in early if k != 1]:
        if k > 0:
            w_copy[2, k].wait_recv()
        own, relay = spread(dx, k, down_piece(k), dx_s, dx_r)
        own()
        if k > 0:
            w_copy[2, k].wait_send()
            w_copy[1, k].start()
        advance(relay, 1)
    for k in late:
        w_copy[0, k].wait_send()
        w_copy[2, k].start()
    advance(lambda: None, 0)
    for k in range(tp_n):
        fx[k, 1].wait_recv()
        fx[k, 2].wait_recv()

    def pair_columns(pair):
        base = tp_peer[pair] - lax.rem(tp_peer[pair], 2)
        return pl.ds(pl.multiple_of(base * width, 2 * width), 2 * width)

    def pair_product(b, at):
        x = xrows[b, :, :, at].reshape(block, 2 * width)
        gate = lax.dot_general(x, gate_out[:, at], NT, preferred_element_type=jnp.float32)
        up = lax.dot_general(x, up_out[:, at], NT, preferred_element_type=jnp.float32)
        return gate, up

    for pair in pairs[:-1]:
        for k in (pair, pair + 1):
            if k > 0:
                w_copy[0, k].wait_recv()
                w_copy[1, k].wait_recv()
        at = pair_columns(pair)

        @pl.loop(0, fs_n)
        def _(b):
            gate, up = pair_product(b, at)
            if pair > 0:
                gate = gate + acc[b, :, :flat]
                up = up + acc[b, :, flat:]
            acc[b, :, :flat] = gate
            acc[b, :, flat:] = up

    for k in (pairs[-1], pairs[-1] + 1):
        w_copy[0, k].wait_recv()
        w_copy[1, k].wait_recv()
    h_copy = {}
    own_units = pl.ds(pl.multiple_of(f * flat, flat), flat)
    for j in (3, 1, 2, 0):
        b = fs_peer[j]
        gate, up = pair_product(b, pair_columns(pairs[-1]))
        gate = gate + acc[b, :, :flat]
        up = up + acc[b, :, flat:]
        active = gate / (1.0 + jnp.exp(-gate)) * up
        route = xrows[b, :, :, model:].reshape(block, LANES).astype(jnp.float32)
        for e in range(experts):
            at = slice(e * units, (e + 1) * units)
            hid[j, :, at] = (route[:, e : e + 1] * active[:, at]).astype(jnp.bfloat16)
        if j > 0:
            h_copy[j] = remote(
                hid.at[j], hcat.at[:, own_units], h_s.at[j], h_r.at[j], b, t
            )
            h_copy[j].start()
        else:
            hcat[:, own_units] = hid[j]
    for copy in h_copy.values():
        copy.wait_recv()

    ret_copy = {}

    def give_back(pair):
        for k in (pair, pair + 1):
            dx[k, 1].wait_recv()
            dx[k, 2].wait_recv()
        at = pair_columns(pair)
        total = jnp.dot(hcat[...], down_all[:, at], preferred_element_type=jnp.float32)
        rsum[pair // 2] = total.astype(jnp.bfloat16).reshape(tp_n, cap, 2 * width)
        for k in near:
            ret_copy[pair, k] = remote(
                rsum.at[pair // 2, tp_peer[k]], ret.at[t, :, at],
                ret_s.at[pair // 2, k], ret_r.at[pair // 2, k], f, tp_peer[k],
            )
            ret_copy[pair, k].start()
        ret[t, :, at] = rsum[pair // 2, t]

    order = [pair for pair in pairs if pair not in late]
    give_back(order[0])
    for k in late:
        w_copy[2, k].wait_recv()
        own, relay = spread(dx, k, down_piece(k), dx_s, dx_r)
        own()
        advance(relay, 2)
    down_kept = pltpu.make_async_copy(down_all.at[own_down], down_out, loc.at[1])
    down_kept.start()
    for pair in order[1:]:
        give_back(pair)
        if pending:
            pending.pop(0)()
    advance(lambda: None, 0)
    give_back(late[0])

    down_kept.wait()
    for copy in ret_copy.values():
        copy.wait_recv()
    for (m, k), copy in w_copy.items():
        if (m == 2 and k in early) or (m == 0 and k in late):
            continue
        copy.wait_send()
    for group in (fx, dx, h_copy, ret_copy):
        for copy in group.values():
            copy.wait_send()


def finish_kernel(
    gate_in, up_in, down_in, ret_ref, placing_ref,
    gate_out, up_out, down_out, mixed_ref, sems,
):
    copies = [
        pltpu.make_async_copy(src, dst, sems.at[i])
        for i, (src, dst) in enumerate(((gate_in, gate_out), (up_in, up_out), (down_in, down_out)))
    ]
    for copy in copies:
        copy.start()
    mixed_ref[...] = lax.dot_general(
        placing_ref[...], ret_ref[...], TN, preferred_element_type=jnp.float32
    ).astype(jnp.bfloat16)
    for copy in copies:
        copy.wait()


def fused_device(fs_n, gate, up, down, prompt, norm_gain, group_pick, route_weight, capacity):
    tp_n, experts, units, width = gate.shape
    tokens, model = prompt.shape
    flat = experts * units
    block = tp_n * capacity
    bf16, f32 = jnp.bfloat16, jnp.float32
    dma = pltpu.SemaphoreType.DMA
    vmem = pl.BlockSpec(memory_space=pltpu.VMEM)
    hbm = pl.BlockSpec(memory_space=pltpu.HBM)
    anywhere = pl.BlockSpec(memory_space=pl.ANY)
    dims = (fs_n, tp_n, experts, units, width, model, capacity)
    served = jax.ShapeDtypeStruct((flat, model), bf16)
    gate_v, up_v, down_v, ret, placing = pl.pallas_call(
        functools.partial(exchange_kernel, dims),
        out_shape=(
            served,
            served,
            served,
            jax.ShapeDtypeStruct((tp_n, capacity, model), bf16),
            jax.ShapeDtypeStruct((block, tokens), bf16),
        ),
        in_specs=[hbm] * 7,
        out_specs=(vmem,) * 5,
        scratch_shapes=[
            pltpu.VMEM((1, width), f32),
            pltpu.VMEM((1, tokens), jnp.int32),
            pltpu.VMEM((experts, tokens), bf16),
            pltpu.VMEM((fs_n * flat, model), bf16),
            pltpu.VMEM((tokens, model), bf16),
            pltpu.VMEM((3, tp_n, flat, width), f32),
            pltpu.VMEM((3, tp_n, flat, width), bf16),
            pltpu.VMEM((tp_n, capacity, model + LANES), bf16),
            pltpu.VMEM((fs_n, tp_n, capacity, model + LANES), bf16),
            pltpu.VMEM((fs_n, block, 2 * flat), f32),
            pltpu.VMEM((fs_n, block, flat), bf16),
            pltpu.VMEM((block, fs_n * flat), bf16),
            pltpu.VMEM((tp_n // 2, tp_n, capacity, 2 * width), bf16),
            pltpu.VMEM((LANES, tokens), bf16),
            dma((4, tp_n)),
            dma((tp_n,)), dma((tp_n,)),
            dma((3, tp_n)), dma((3, tp_n)),
            dma((tp_n, 3)), dma((tp_n, 3)),
            dma((tp_n, 3)), dma((tp_n, 3)),
            dma((fs_n,)), dma((fs_n,)),
            dma((tp_n // 2, tp_n)), dma((tp_n // 2, tp_n)),
            dma((2,)),
        ],
        compiler_params=pltpu.CompilerParams(
            collective_id=0, has_side_effects=True, vmem_limit_bytes=44 * 2**20
        ),
    )(
        *(
            pltpu.with_memory_space_constraint(value, pltpu.HBM)
            for value in (
                prompt,
                norm_gain.reshape(1, width),
                gate.reshape(tp_n, flat, width),
                up.reshape(tp_n, flat, width),
                down.reshape(tp_n, flat, width),
                group_pick.reshape(1, tokens),
                route_weight.T,
            )
        )
    )
    gate_serve, up_serve, down_serve, mixed = pl.pallas_call(
        finish_kernel,
        out_shape=(served, served, served, jax.ShapeDtypeStruct((tokens, model), bf16)),
        in_specs=[anywhere, anywhere, anywhere, vmem, vmem],
        out_specs=(hbm, hbm, hbm, vmem),
        scratch_shapes=[dma((3,))],
        compiler_params=pltpu.CompilerParams(vmem_limit_bytes=16 * 2**20),
    )(gate_v, up_v, down_v, ret.reshape(block, model), placing)
    shape = (1, experts, units, model)
    return gate_serve.reshape(shape), up_serve.reshape(shape), down_serve.reshape(shape), mixed


def per_device(prompt, norm_gain, gate_master, up_master, down_master, group_pick, route_weight):
    group_total = lax.axis_size("tp")
    fs_n = lax.axis_size("fs")
    tok_count = prompt.shape[0]
    capacity = 2 * tok_count // group_total
    slot_total = group_total * capacity
    width, units = gate_master.shape[3], gate_master.shape[2]
    small = group_total == 8 and fs_n == 4
    if small and width % (2 * LANES) == 0 and units % LANES == 0 and capacity % 16 == 0:
        return fused_device(
            fs_n, gate_master, up_master, down_master,
            prompt, norm_gain, group_pick, route_weight, capacity,
        )
    gate_local = (gate_master * norm_gain).astype(jnp.bfloat16)
    up_local = (up_master * norm_gain).astype(jnp.bfloat16)
    down_local = down_master.astype(jnp.bfloat16)
    values = prompt.astype(jnp.float32)
    normed = (values * lax.rsqrt(jnp.mean(values * values, axis=1, keepdims=True) + EPS)).astype(
        jnp.bfloat16
    )
    chosen = group_pick[:, 0]
    member = (chosen[:, None] == jnp.arange(group_total, dtype=jnp.int32)[None, :]).astype(
        jnp.int32
    )
    slot_rank = jnp.sum(jnp.cumsum(member, axis=0) * member, axis=1) - 1
    target = chosen * capacity + slot_rank
    placing = (jnp.arange(slot_total, dtype=jnp.int32)[:, None] == target[None, :]).astype(
        jnp.bfloat16
    )
    gate_serve, up_serve, down_serve = (
        lax.all_to_all(gate_local, "tp", split_axis=0, concat_axis=3, tiled=True),
        lax.all_to_all(up_local, "tp", split_axis=0, concat_axis=3, tiled=True),
        lax.all_to_all(down_local, "tp", split_axis=0, concat_axis=3, tiled=True),
    )
    send_rows = jnp.dot(placing, normed, preferred_element_type=jnp.float32).astype(jnp.bfloat16)
    send_weights = jnp.dot(placing, route_weight, preferred_element_type=jnp.float32).astype(
        jnp.bfloat16
    )
    got_rows, got_weights = (
        lax.all_to_all(
            send_rows.reshape(group_total, capacity, -1),
            "tp",
            split_axis=0,
            concat_axis=0,
            tiled=True,
        ),
        lax.all_to_all(
            send_weights.reshape(group_total, capacity, -1),
            "tp",
            split_axis=0,
            concat_axis=0,
            tiled=True,
        ),
    )
    group_rows = got_rows.reshape(slot_total, -1)
    weights = got_weights.reshape(slot_total, -1)
    gathered = (
        lax.all_gather(gate_serve, "fs", axis=2, tiled=True),
        lax.all_gather(up_serve, "fs", axis=2, tiled=True),
        lax.all_gather(down_serve, "fs", axis=2, tiled=True),
    )
    summed = expert_rows(group_rows, weights, gathered)
    result = summed.astype(jnp.bfloat16).reshape(group_total, capacity, -1)
    returned = lax.all_to_all(result, "tp", split_axis=0, concat_axis=0, tiled=True)
    mixed = jnp.einsum(
        "st,sd->td", placing, returned.reshape(slot_total, -1), preferred_element_type=jnp.float32
    ).astype(jnp.bfloat16)
    return (gate_serve, up_serve, down_serve, mixed)


def solution(mesh):
    placed = (
        P(("fs", "tp"), None),
        P("tp"),
        P(None, None, "fs", "tp"),
        P(None, None, "fs", "tp"),
        P(None, None, "fs", "tp"),
        P(("fs", "tp"), None),
        P(("fs", "tp"), None),
    )
    return jax.shard_map(
        per_device,
        mesh=mesh,
        in_specs=placed,
        out_specs=(
            P("tp", None, "fs", None),
            P("tp", None, "fs", None),
            P("tp", None, "fs", None),
            P(("fs", "tp"), None),
        ),
        check_vma=False,
    )
```

time: 156 us -> 128 us (0.82)
  Pallas kernels: 139 us -> 128 us
  other arithmetic: 8.54 us -> 0 us
  local copies, waits for them, and re-layouts: 6.21 us -> 0 us
    pallas_call x1, Pallas kernels: 139 us -> 125 us  [fused_device(): pl.pallas_call(functools.partial(exchange_kernel, dims), out_shape=(serve...]
    unnamed x19 -> x0, local copies, waits for them, and re-layouts: 6.21 us -> none
    convert_element_type x5 -> x0, other arithmetic: 5.49 us -> none  [the longest x1 1.81 us: per_device(): up_local = (up_master * norm_gain).astype(jnp.bfloat16)]
    pallas_call x0 -> x1, Pallas kernels: none -> 2.51 us  [fused_device(): pl.pallas_call(finish_kernel, out_shape=(served, served, served, jax.Shap...]
    reduce_sum x2 -> x0, other arithmetic: 2.2 us -> none  [the longest x1 1.38 us: per_device(): jnp.mean(values * values, axis=1, keepdims=True) + EPS]
where the time goes in v1:
time: 128 us
  Pallas kernels  128 us (100%)
    pallas_call x1, Pallas kernels, fused_device(): pl.pallas_call(functools.partial(exchange_kernel, dims), out_shape=(serve...  125 us

profile of v1, /device:TPU:0, one launch (start us, length us, event | category | flops | bytes accessed | tf_op | source)
XLA Modules:
  0.0 128.2 jit_solution(1573623370340249481)
XLA Ops:
  0.6 125.0 %shard_map.102 = (bf16[256,2048]{1,0:T(8,128)(2,1)S(1)}, bf16[256,2048]{1,0:T(8,128)(2,1)S(1)}, bf16[256,2048]{1,0:T(8,128)(2,1)S(1)}, bf16[8,32,2048]{2,1,0:T(8,128)(2,1)S(1)}, bf16[256,128]{1,0:T(8,128)(2,1)S(1)}) custom-call(bf16[128,2048]{1,0:T(8,128)(2,1)} %prompt_in.1, f32[1,256]{1,0:T(1,128)} %bitcast.14, f32[8,256,256]{2,1,0:T(8,128)} %bitcast.11, ...), custom_call_target="tpu_custom_call" | custom-call | tf_op jit(solution)/shard_map/pallas_call | solution.py:383
  125.7 2.5 %shard_map.103 = (bf16[256,2048]{1,0:T(8,128)(2,1)}, bf16[256,2048]{1,0:T(8,128)(2,1)}, bf16[256,2048]{1,0:T(8,128)(2,1)}, bf16[128,2048]{1,0:T(8,128)(2,1)}) custom-call(bf16[256,2048]{1,0:T(8,128)(2,1)S(1)} %get-tuple-element.13.gate_in, bf16[256,2048]{1,0:T(8,128)(2,1)S(1)} %get-tuple-element.14.up_in, bf16[256,2048]{1,0:T(8,128)(2,1)S(1)} %get-tuple-element.15.down_in, ...), custom_call_target="tpu_custom_call" | custom-call | tf_op jit(solution)/shard_map/pallas_call | solution.py:435

commit v2 on v1

--- a/solution.py
+++ b/solution.py
@@ -42,12 +42,33 @@
     return total
 
 
+class Transfer:
+    def __init__(self, copy, log):
+        self.copy, self.log, self.sent, self.got = copy, log, False, False
+
+    def start(self):
+        self.log.append(self)
+        self.copy.start()
+
+    def wait_send(self):
+        if not self.sent:
+            self.sent = True
+            self.copy.wait_send()
+
+    def wait_recv(self):
+        if not self.got:
+            self.got = True
+            self.copy.wait_recv()
+
+
 def exchange_kernel(
     dims,
     prompt_in, gain_in, gate_in, up_in, down_in, pick_in, route_in,
     gate_out, up_out, down_out, ret, placing_ref,
-    gain_ref, pick_ref, route_ref, down_all, prompt, stage, wsend, rows, xrows, acc, hid, hcat, rsum, route_pad,
-    load, rows_s, rows_r, w_s, w_r, fx_s, fx_r, dx_s, dx_r, h_s, h_r, ret_s, ret_r, loc,
+    gain_ref, pick_ref, route_ref, down_all, prompt, stage, wsend, rows, xrows, acc, hid, hcat,
+    rsum, route_send, route_all,
+    load, rows_s, rows_r, w_s, w_r, fx_s, fx_r, dx_s, dx_r, h_s, h_r, ret_s, ret_r,
+    rt_s, rt_r, rx_s, rx_r, loc,
 ):
     fs_n, tp_n, experts, units, width, model, cap = dims
     flat, block, tokens = experts * units, tp_n * cap, prompt.shape[0]
@@ -57,40 +78,48 @@
     fs_peer = [flipped(f, j, fs_n) for j in range(fs_n)]
 
     near = list(range(2, tp_n)) + [1]
-    late = [tp_n // 2, tp_n // 2 + 1]
-    early = [k for k in near if k not in late]
+    late = list(range(tp_n // 2, tp_n))
+    far_first = late + [k for k in near if k not in late]
+    fill = tp_n - 2
     pairs = list(range(0, tp_n, 2))
-    down_order = early + late
-
-    prompt_load = pltpu.make_async_copy(prompt_in, prompt, load.at[3, 0])
+    gate_m, up_m, down_m, rows_m = 0, 1, 2, 3
+    plan = {}
+    for k in near:
+        if k in late:
+            plan[k] = [rows_m, gate_m, up_m, down_m]
+        else:
+            plan[k] = [rows_m, down_m, gate_m, up_m]
+    plan[fill] = [gate_m, rows_m, up_m, down_m]
+    plan[1] = [down_m, rows_m, gate_m, up_m]
+
+    sources = (gate_in, up_in, down_in)
+    loads = {}
+
+    def load_weight(m, k):
+        loads[m, k] = pltpu.make_async_copy(
+            sources[m].at[tp_peer[k]], stage.at[m, k], load.at[m, k]
+        )
+        loads[m, k].start()
+
     small_loads = [
         pltpu.make_async_copy(src, dst, load.at[3, 1 + i])
         for i, (src, dst) in enumerate(
-            ((pick_in, pick_ref), (route_in, route_ref), (gain_in, gain_ref))
+            ((gain_in, gain_ref), (pick_in, pick_ref), (route_in, route_ref))
         )
     ]
     for copy in small_loads:
         copy.start()
+    load_weight(gate_m, fill)
+    load_weight(down_m, 0)
+    load_weight(down_m, 1)
+    prompt_load = pltpu.make_async_copy(prompt_in, prompt, load.at[3, 0])
     prompt_load.start()
-    sources = (gate_in, up_in, down_in)
-    loads = {}
-
-    def load_weight(m, k):
-        loads[m, k] = pltpu.make_async_copy(
-            sources[m].at[tp_peer[k]], stage.at[m, k], load.at[m, k]
-        )
-        loads[m, k].start()
-
-    for k in early:
-        load_weight(2, k)
-    for m in range(2):
-        for k in near:
-            load_weight(m, k)
-    for k in late:
-        load_weight(2, k)
-    for m in range(3):
-        load_weight(m, 0)
-
+    for m in (down_m, gate_m, up_m):
+        for k in range(tp_n):
+            if (m, k) not in loads:
+                load_weight(m, k)
+
+    started = []
     barrier = pltpu.get_barrier_semaphore()
     for k in range(1, tp_n):
         pl.semaphore_signal(barrier, inc=1, device_id=(f, tp_peer[k]), device_id_type=MESH)
@@ -100,14 +129,84 @@
     def columns(index):
         return pl.ds(pl.multiple_of(index * width, width), width)
 
+    def own_rows_of(owner):
+        return pl.ds(pl.multiple_of(owner * flat, flat), flat)
+
     def remote(src, dst, send, recv, fs_to, tp_to):
-        return pltpu.make_async_remote_copy(
+        copy = pltpu.make_async_remote_copy(
             src_ref=src, dst_ref=dst, send_sem=send, recv_sem=recv,
             device_id=(fs_to, tp_to), device_id_type=MESH,
         )
+        return Transfer(copy, started)
+
+    copies = {}
+    landing = (
+        gate_out.at[:, columns(t)],
+        up_out.at[:, columns(t)],
+        down_all.at[own_rows_of(f), columns(t)],
+    )
+    for k in near:
+        for m in (gate_m, up_m, down_m):
+            copies[m, k] = remote(
+                wsend.at[m, k], landing[m], w_s.at[m, k], w_r.at[m, k], f, tp_peer[k]
+            )
+        copies[rows_m, k] = remote(
+            rows.at[tp_peer[k]], xrows.at[f, t], rows_s.at[k], rows_r.at[k], f, tp_peer[k]
+        )
+
+    def convert(m, k):
+        loads[m, k].wait()
+        value = stage[m, k]
+        if m != down_m:
+            value = value * gain_ref[...]
+        value = value.astype(jnp.bfloat16)
+        if k > 0:
+            wsend[m, k] = value
+        elif m == down_m:
+            down_all[own_rows_of(f), columns(t)] = value
+        else:
+            (gate_out, up_out)[m][:, columns(t)] = value
+
+    def spread(log, k, piece, send, recv):
+        first, second = (1, 2) if (k // 2 + k) % 2 == 0 else (2, 1)
+
+        def go(slot, owner, to):
+            ref = piece(owner)
+            log[k, slot] = remote(ref, ref, send.at[k, slot], recv.at[k, slot], fs_peer[to], t)
+            log[k, slot].start()
+
+        go(0, f, first)
+        go(1, f, second)
+
+        def relay():
+            log[k, 0].wait_recv()
+            go(2, fs_peer[first], second)
+
+        return relay
+
+    fx, dx = {}, {}
+
+    def spread_rows(k):
+        return spread(fx, k, lambda owner: xrows.at[owner, tp_peer[k]], fx_s, fx_r)
+
+    def spread_down(k):
+        return spread(
+            dx, k, lambda owner: down_all.at[own_rows_of(owner), columns(tp_peer[k])], dx_s, dx_r
+        )
+
+    pending = []
+
+    def advance(lag, relay=None):
+        if relay is not None:
+            pending.append(relay)
+        while len(pending) > lag:
+            pending.pop(0)()
 
     for copy in small_loads:
         copy.wait()
+    convert(gate_m, fill)
+    convert(down_m, 1)
+    convert(down_m, 0)
     pick = pick_ref[...].astype(jnp.float32)
     group_id = lax.broadcasted_iota(jnp.int32, (tp_n, tokens), 0).astype(jnp.float32)
     member = jnp.where(group_id == pick, 1.0, 0.0)
@@ -122,138 +221,84 @@
     slot = lax.broadcasted_iota(jnp.int32, (block, tokens), 0).astype(jnp.float32)
     placing = jnp.where(slot == target, 1.0, 0.0).astype(jnp.bfloat16)
     placing_ref[...] = placing
-    route_pad[...] = jnp.zeros_like(route_pad)
-    route_pad[0:experts, :] = route_ref[...]
-    routed = lax.dot_general(placing, route_pad[...], NT, preferred_element_type=jnp.float32)
-    rows[:, :, model:] = routed.astype(jnp.bfloat16).reshape(tp_n, cap, LANES)
+
+    pl.semaphore_wait(barrier, tp_n - 1 + fs_n - 1)
+    copies[gate_m, fill].start()
+    copies[down_m, 1].start()
+    advance(1, spread_down(0))
+
     prompt_load.wait()
     values = prompt[...].astype(jnp.float32)
     scale = lax.rsqrt(jnp.mean(values * values, axis=1, keepdims=True) + EPS)
     normed = (values * scale).astype(jnp.bfloat16)
-    rows[:, :, :model] = (
+    rows[...] = (
         jnp.dot(placing, normed, preferred_element_type=jnp.float32)
         .astype(jnp.bfloat16)
         .reshape(tp_n, cap, model)
     )
-
-    pl.semaphore_wait(barrier, tp_n - 1 + fs_n - 1)
-
-    rows_copy = {}
-    for k in near:
-        rows_copy[k] = remote(
-            rows.at[tp_peer[k]], xrows.at[f, t], rows_s.at[k], rows_r.at[k], f, tp_peer[k]
-        )
-        rows_copy[k].start()
+    for k in near:
+        copies[rows_m, k].start()
     own_rows = pltpu.make_async_copy(rows.at[t], xrows.at[f, t], loc.at[0])
     own_rows.start()
-
-    own_down = pl.ds(pl.multiple_of(f * flat, flat), flat)
-
-    def landing(m):
-        if m == 2:
-            return down_all.at[own_down, columns(t)]
-        return (gate_out, up_out)[m].at[:, columns(t)]
-
-    w_copy = {}
-
-    def convert(m, k):
-        loads[m, k].wait()
-        value = stage[m, k]
-        if m < 2:
-            value = value * gain_ref[...]
-        value = value.astype(jnp.bfloat16)
-        if k > 0:
-            wsend[m, k] = value
-            w_copy[m, k] = remote(
-                wsend.at[m, k], landing(m), w_s.at[m, k], w_r.at[m, k], f, tp_peer[k]
-            )
-        elif m == 2:
-            down_all[own_down, columns(t)] = value
-        else:
-            (gate_out, up_out)[m][:, columns(t)] = value
-
-    for k in early:
-        convert(2, k)
-    for k in early:
-        w_copy[2, k].start()
-    for k in near:
-        convert(0, k)
-    for k in late:
-        w_copy[0, k].start()
-    for m in range(3):
-        convert(m, 0)
-
-    def spread(copies, k, piece, send, recv):
-        first, second = (1, 2) if (k // 2 + k) % 2 == 0 else (2, 1)
-        origin = {0: f, 1: fs_peer[first], 2: fs_peer[second]}
-
-        def go(slot, owner, to):
-            ref = piece(owner)
-            copies[k, slot] = remote(
-                ref, ref, send.at[k, slot], recv.at[k, slot], fs_peer[to], t
-            )
-            copies[k, slot].start()
-
-        def own():
-            go(0, f, first)
-            go(1, f, second)
-
-        def relay():
-            copies[k, 0].wait_recv()
-            go(2, fs_peer[first], second)
-
-        return own, relay
-
-    fx, dx = {}, {}
-
-    def rows_piece(k):
-        return lambda owner: xrows.at[owner, tp_peer[k]]
-
-    def down_piece(k):
-        return lambda owner: down_all.at[
-            pl.ds(pl.multiple_of(owner * flat, flat), flat), columns(tp_peer[k])
-        ]
-
-    pending = []
-
-    def advance(relay, lag):
-        pending.append(relay)
-        while len(pending) > lag:
-            pending.pop(0)()
-
+    route_send[...] = jnp.zeros_like(route_send)
+    for g in range(tp_n):
+        route_send[g, :, :cap] = lax.dot_general(
+            route_ref[...], placing_ref[g * cap : (g + 1) * cap, :], NT,
+            preferred_element_type=jnp.float32,
+        )
+    route_copy = {}
+    for k in near:
+        route_copy[k] = remote(
+            route_send.at[tp_peer[k]], route_all.at[f, t], rt_s.at[k], rt_r.at[k], f, tp_peer[k]
+        )
+        route_copy[k].start()
+    route_all[f, t] = route_send[t]
+
+    for k in near:
+        m = plan[k][1]
+        if k != 1 and m != rows_m:
+            convert(m, k)
+            copies[m, k].start()
+    for k in near:
+        m = plan[k][2]
+        convert(m, k)
+    convert(gate_m, 0)
+    convert(up_m, 0)
+
+    copies[down_m, 1].wait_recv()
+    advance(1, spread_down(1))
     own_rows.wait()
     for k in [0, 1] + near[:-1]:
         if k > 0:
-            rows_copy[k].wait_recv()
-        own, relay = spread(fx, k, rows_piece(k), fx_s, fx_r)
-        own()
-        if k in early:
-            rows_copy[k].wait_send()
-            w_copy[0, k].start()
+            copies[rows_m, k].wait_recv()
+        advance(1, spread_rows(k))
         if k > 0:
-            convert(1, k)
-        if k in late:
-            rows_copy[k].wait_send()
-            w_copy[1, k].start()
-        advance(relay, 1)
-    for k in late:
-        convert(2, k)
-    for k in [0, 1] + [k for k in early if k != 1]:
-        if k > 0:
-            w_copy[2, k].wait_recv()
-        own, relay = spread(dx, k, down_piece(k), dx_s, dx_r)
-        own()
-        if k > 0:
-            w_copy[2, k].wait_send()
-            w_copy[1, k].start()
-        advance(relay, 1)
-    for k in late:
-        w_copy[0, k].wait_send()
-        w_copy[2, k].start()
-    advance(lambda: None, 0)
+            copies[plan[k][0], k].wait_send()
+            copies[plan[k][2], k].start()
+            convert(plan[k][3], k)
+    for k in range(2, tp_n):
+        if k not in late:
+            copies[down_m, k].wait_recv()
+            advance(1, spread_down(k))
+    for k in near:
+        copies[plan[k][1], k].wait_send()
+        if k not in late:
+            copies[plan[k][3], k].start()
+    advance(0)
+    for k in near:
+        route_copy[k].wait_recv()
+    route_spread = []
+    for j in range(1, fs_n):
+        copy = remote(
+            route_all.at[f], route_all.at[f], rx_s.at[j], rx_r.at[j], fs_peer[j], t
+        )
+        copy.start()
+        route_spread.append(copy)
     for k in range(tp_n):
         fx[k, 1].wait_recv()
         fx[k, 2].wait_recv()
+    for copy in route_spread:
+        copy.wait_recv()
 
     def pair_columns(pair):
         base = tp_peer[pair] - lax.rem(tp_peer[pair], 2)
@@ -266,10 +311,14 @@
         return gate, up
 
     for pair in pairs[:-1]:
+        if pair == late[0]:
+            for k in late:
+                copies[up_m, k].wait_send()
+                copies[down_m, k].start()
         for k in (pair, pair + 1):
             if k > 0:
-                w_copy[0, k].wait_recv()
-                w_copy[1, k].wait_recv()
+                copies[gate_m, k].wait_recv()
+                copies[up_m, k].wait_recv()
         at = pair_columns(pair)
 
         @pl.loop(0, fs_n)
@@ -282,29 +331,28 @@
             acc[b, :, flat:] = up
 
     for k in (pairs[-1], pairs[-1] + 1):
-        w_copy[0, k].wait_recv()
-        w_copy[1, k].wait_recv()
+        copies[gate_m, k].wait_recv()
+        copies[up_m, k].wait_recv()
     h_copy = {}
-    own_units = pl.ds(pl.multiple_of(f * flat, flat), flat)
     for j in (3, 1, 2, 0):
         b = fs_peer[j]
         gate, up = pair_product(b, pair_columns(pairs[-1]))
         gate = gate + acc[b, :, :flat]
         up = up + acc[b, :, flat:]
         active = gate / (1.0 + jnp.exp(-gate)) * up
-        route = xrows[b, :, :, model:].reshape(block, LANES).astype(jnp.float32)
-        for e in range(experts):
-            at = slice(e * units, (e + 1) * units)
-            hid[j, :, at] = (route[:, e : e + 1] * active[:, at]).astype(jnp.bfloat16)
+        for s in range(tp_n):
+            line = slice(s * cap, (s + 1) * cap)
+            route = jnp.transpose(route_all[b, s])
+            for e in range(experts):
+                at = slice(e * units, (e + 1) * units)
+                hid[j, line, at] = (route[:cap, e : e + 1] * active[line, at]).astype(jnp.bfloat16)
         if j > 0:
             h_copy[j] = remote(
-                hid.at[j], hcat.at[:, own_units], h_s.at[j], h_r.at[j], b, t
+                hid.at[j], hcat.at[:, own_rows_of(f)], h_s.at[j], h_r.at[j], b, t
             )
             h_copy[j].start()
         else:
-            hcat[:, own_units] = hid[j]
-    for copy in h_copy.values():
-        copy.wait_recv()
+            hcat[:, own_rows_of(f)] = hid[j]
 
     ret_copy = {}
 
@@ -315,7 +363,7 @@
         at = pair_columns(pair)
         total = jnp.dot(hcat[...], down_all[:, at], preferred_element_type=jnp.float32)
         rsum[pair // 2] = total.astype(jnp.bfloat16).reshape(tp_n, cap, 2 * width)
-        for k in near:
+        for k in far_first:
             ret_copy[pair, k] = remote(
                 rsum.at[pair // 2, tp_peer[k]], ret.at[t, :, at],
                 ret_s.at[pair // 2, k], ret_r.at[pair // 2, k], f, tp_peer[k],
@@ -323,37 +371,34 @@
             ret_copy[pair, k].start()
         ret[t, :, at] = rsum[pair // 2, t]
 
-    order = [pair for pair in pairs if pair not in late]
-    give_back(order[0])
-    for k in late:
-        w_copy[2, k].wait_recv()
-        own, relay = spread(dx, k, down_piece(k), dx_s, dx_r)
-        own()
-        advance(relay, 2)
-    down_kept = pltpu.make_async_copy(down_all.at[own_down], down_out, loc.at[1])
+    for k in late[:2]:
+        copies[down_m, k].wait_recv()
+        advance(1, spread_down(k))
+    for copy in h_copy.values():
+        copy.wait_recv()
+    for pair in pairs:
+        if pair not in late:
+            give_back(pair)
+    for k in late[2:]:
+        copies[down_m, k].wait_recv()
+        advance(1, spread_down(k))
+    advance(0)
+    down_kept = pltpu.make_async_copy(down_all.at[own_rows_of(f)], down_out, loc.at[1])
     down_kept.start()
-    for pair in order[1:]:
-        give_back(pair)
-        if pending:
-            pending.pop(0)()
-    advance(lambda: None, 0)
-    give_back(late[0])
+    for pair in pairs:
+        if pair in late:
+            give_back(pair)
 
     down_kept.wait()
     for copy in ret_copy.values():
         copy.wait_recv()
-    for (m, k), copy in w_copy.items():
-        if (m == 2 and k in early) or (m == 0 and k in late):
-            continue
+    for copy in started:
         copy.wait_send()
-    for group in (fx, dx, h_copy, ret_copy):
-        for copy in group.values():
-            copy.wait_send()
 
 
 def finish_kernel(
     gate_in, up_in, down_in, ret_ref, placing_ref,
-    gate_out, up_out, down_out, mixed_ref, sems,
+    gate_out, up_out, down_out, mixed_out, mixed, sems, mixed_sems,
 ):
     copies = [
         pltpu.make_async_copy(src, dst, sems.at[i])
@@ -361,9 +406,16 @@
     ]
     for copy in copies:
         copy.start()
-    mixed_ref[...] = lax.dot_general(
-        placing_ref[...], ret_ref[...], TN, preferred_element_type=jnp.float32
-    ).astype(jnp.bfloat16)
+    parts = mixed_sems.shape[0]
+    step = mixed.shape[1] // parts
+    for i in range(parts):
+        at = slice(i * step, (i + 1) * step)
+        mixed[:, at] = lax.dot_general(
+            placing_ref[...], ret_ref[:, at], TN, preferred_element_type=jnp.float32
+        ).astype(jnp.bfloat16)
+        copy = pltpu.make_async_copy(mixed.at[:, at], mixed_out.at[:, at], mixed_sems.at[i])
+        copy.start()
+        copies.append(copy)
     for copy in copies:
         copy.wait()
 
@@ -399,13 +451,14 @@
             pltpu.VMEM((tokens, model), bf16),
             pltpu.VMEM((3, tp_n, flat, width), f32),
             pltpu.VMEM((3, tp_n, flat, width), bf16),
-            pltpu.VMEM((tp_n, capacity, model + LANES), bf16),
-            pltpu.VMEM((fs_n, tp_n, capacity, model + LANES), bf16),
+            pltpu.VMEM((tp_n, capacity, model), bf16),
+            pltpu.VMEM((fs_n, tp_n, capacity, model), bf16),
             pltpu.VMEM((fs_n, block, 2 * flat), f32),
             pltpu.VMEM((fs_n, block, flat), bf16),
             pltpu.VMEM((block, fs_n * flat), bf16),
             pltpu.VMEM((tp_n // 2, tp_n, capacity, 2 * width), bf16),
-            pltpu.VMEM((LANES, tokens), bf16),
+            pltpu.VMEM((tp_n, experts, LANES), f32),
+            pltpu.VMEM((fs_n, tp_n, experts, LANES), f32),
             dma((4, tp_n)),
             dma((tp_n,)), dma((tp_n,)),
             dma((3, tp_n)), dma((3, tp_n)),
@@ -413,6 +466,8 @@
             dma((tp_n, 3)), dma((tp_n, 3)),
             dma((fs_n,)), dma((fs_n,)),
             dma((tp_n // 2, tp_n)), dma((tp_n // 2, tp_n)),
+            dma((tp_n,)), dma((tp_n,)),
+            dma((fs_n,)), dma((fs_n,)),
             dma((2,)),
         ],
         compiler_params=pltpu.CompilerParams(
@@ -436,8 +491,8 @@
         finish_kernel,
         out_shape=(served, served, served, jax.ShapeDtypeStruct((tokens, model), bf16)),
         in_specs=[anywhere, anywhere, anywhere, vmem, vmem],
-        out_specs=(hbm, hbm, hbm, vmem),
-        scratch_shapes=[dma((3,))],
+        out_specs=(hbm,) * 4,
+        scratch_shapes=[pltpu.VMEM((tokens, model), bf16), dma((3,)), dma((4,))],
         compiler_params=pltpu.CompilerParams(vmem_limit_bytes=16 * 2**20),
     )(gate_v, up_v, down_v, ret.reshape(block, model), placing)
     shape = (1, experts, units, model)

time: 128 us -> 124 us (0.969)
  Pallas kernels: 128 us -> 123 us
    pallas_call x1, Pallas kernels: 125 us -> 121 us  [fused_device(): pl.pallas_call(functools.partial(exchange_kernel, dims), out_shape=(serve...]
where the time goes in v2:
time: 124 us
  Pallas kernels  123 us (99%)
    pallas_call x1, Pallas kernels, fused_device(): pl.pallas_call(functools.partial(exchange_kernel, dims), out_shape=(serve...  121 us

profile of v2, /device:TPU:0, one launch (start us, length us, event | category | flops | bytes accessed | tf_op | source)
XLA Modules:
  0.0 123.8 jit_solution(6847605847185590623)
XLA Ops:
  0.6 121.3 %shard_map.102 = (bf16[256,2048]{1,0:T(8,128)(2,1)S(1)}, bf16[256,2048]{1,0:T(8,128)(2,1)S(1)}, bf16[256,2048]{1,0:T(8,128)(2,1)S(1)}, bf16[8,32,2048]{2,1,0:T(8,128)(2,1)S(1)}, bf16[256,128]{1,0:T(8,128)(2,1)S(1)}) custom-call(bf16[128,2048]{1,0:T(8,128)(2,1)} %prompt_in.1, f32[1,256]{1,0:T(1,128)} %bitcast.14, f32[8,256,256]{2,1,0:T(8,128)} %bitcast.11, ...), custom_call_target="tpu_custom_call" | custom-call | tf_op jit(solution)/shard_map/pallas_call | solution.py:435
  121.9 1.9 %shard_map.103 = (bf16[256,2048]{1,0:T(8,128)(2,1)}, bf16[256,2048]{1,0:T(8,128)(2,1)}, bf16[256,2048]{1,0:T(8,128)(2,1)}, bf16[128,2048]{1,0:T(8,128)(2,1)}) custom-call(bf16[256,2048]{1,0:T(8,128)(2,1)S(1)} %get-tuple-element.13.gate_in, bf16[256,2048]{1,0:T(8,128)(2,1)S(1)} %get-tuple-element.14.up_in, bf16[256,2048]{1,0:T(8,128)(2,1)S(1)} %get-tuple-element.15.down_in, ...), custom_call_target="tpu_custom_call" | custom-call | tf_op jit(solution)/shard_map/pallas_call | solution.py:490

commit v3 on v2

--- a/solution.py
+++ b/solution.py
@@ -68,7 +68,7 @@
     gain_ref, pick_ref, route_ref, down_all, prompt, stage, wsend, rows, xrows, acc, hid, hcat,
     rsum, route_send, route_all,
     load, rows_s, rows_r, w_s, w_r, fx_s, fx_r, dx_s, dx_r, h_s, h_r, ret_s, ret_r,
-    rt_s, rt_r, rx_s, rx_r, loc,
+    rt_s, rt_r, rx_s, rx_r, loc, ready,
 ):
     fs_n, tp_n, experts, units, width, model, cap = dims
     flat, block, tokens = experts * units, tp_n * cap, prompt.shape[0]
@@ -80,7 +80,8 @@
     near = list(range(2, tp_n)) + [1]
     late = list(range(tp_n // 2, tp_n))
     far_first = late + [k for k in near if k not in late]
-    fill = tp_n - 2
+    fill = [tp_n - 2, tp_n - 1]
+    inner = lax.rem(lax.div(lax.div(t, 2) + 1, 2), 2)
     pairs = list(range(0, tp_n, 2))
     gate_m, up_m, down_m, rows_m = 0, 1, 2, 3
     plan = {}
@@ -89,7 +90,8 @@
             plan[k] = [rows_m, gate_m, up_m, down_m]
         else:
             plan[k] = [rows_m, down_m, gate_m, up_m]
-    plan[fill] = [gate_m, rows_m, up_m, down_m]
+    for k in fill:
+        plan[k] = [gate_m, rows_m, up_m, down_m]
     plan[1] = [down_m, rows_m, gate_m, up_m]
 
     sources = (gate_in, up_in, down_in)
@@ -109,7 +111,8 @@
     ]
     for copy in small_loads:
         copy.start()
-    load_weight(gate_m, fill)
+    for k in fill:
+        load_weight(gate_m, k)
     load_weight(down_m, 0)
     load_weight(down_m, 1)
     prompt_load = pltpu.make_async_copy(prompt_in, prompt, load.at[3, 0])
@@ -121,10 +124,19 @@
 
     started = []
     barrier = pltpu.get_barrier_semaphore()
-    for k in range(1, tp_n):
-        pl.semaphore_signal(barrier, inc=1, device_id=(f, tp_peer[k]), device_id_type=MESH)
-    for j in range(1, fs_n):
-        pl.semaphore_signal(barrier, inc=1, device_id=(fs_peer[j], t), device_id_type=MESH)
+
+    def greet(sem, fs_to, tp_to):
+        pl.semaphore_signal(sem, inc=1, device_id=(fs_to, tp_to), device_id_type=MESH)
+
+    for k in (2, 3, 1):
+        greet(barrier, f, tp_peer[k])
+    for j in (1, 2):
+        greet(barrier, fs_peer[j], t)
+
+    @pl.when(inner == 1)
+    def _():
+        for k in fill:
+            greet(barrier, f, tp_peer[k])
 
     def columns(index):
         return pl.ds(pl.multiple_of(index * width, width), width)
@@ -204,9 +216,23 @@
 
     for copy in small_loads:
         copy.wait()
-    convert(gate_m, fill)
+    for k in fill:
+        convert(gate_m, k)
+
+    pl.semaphore_wait(barrier, 5 + 2 * inner)
+
+    @pl.when(inner == 1)
+    def _():
+        greet(ready.at[0], f, tp_peer[fill[0]])
+        greet(ready.at[0], f, tp_peer[2])
+        for k in fill:
+            copies[gate_m, k].start()
+
     convert(down_m, 1)
     convert(down_m, 0)
+    copies[down_m, 1].start()
+    advance(1, spread_down(0))
+
     pick = pick_ref[...].astype(jnp.float32)
     group_id = lax.broadcasted_iota(jnp.int32, (tp_n, tokens), 0).astype(jnp.float32)
     member = jnp.where(group_id == pick, 1.0, 0.0)
@@ -222,10 +248,10 @@
     placing = jnp.where(slot == target, 1.0, 0.0).astype(jnp.bfloat16)
     placing_ref[...] = placing
 
-    pl.semaphore_wait(barrier, tp_n - 1 + fs_n - 1)
-    copies[gate_m, fill].start()
-    copies[down_m, 1].start()
-    advance(1, spread_down(0))
+    @pl.when(inner == 1)
+    def _():
+        pl.semaphore_wait(ready.at[0], 1)
+        greet(ready.at[1], f, tp_peer[2])
 
     prompt_load.wait()
     values = prompt[...].astype(jnp.float32)
@@ -237,6 +263,17 @@
         .reshape(tp_n, cap, model)
     )
     for k in near:
+        if k not in late:
+            copies[rows_m, k].start()
+
+    @pl.when(inner == 0)
+    def _():
+        pl.semaphore_wait(ready.at[0], 1)
+        pl.semaphore_wait(ready.at[1], 1)
+        for k in fill:
+            copies[gate_m, k].start()
+
+    for k in late:
         copies[rows_m, k].start()
     own_rows = pltpu.make_async_copy(rows.at[t], xrows.at[f, t], loc.at[0])
     own_rows.start()
@@ -360,16 +397,16 @@
         for k in (pair, pair + 1):
             dx[k, 1].wait_recv()
             dx[k, 2].wait_recv()
-        at = pair_columns(pair)
+        at, part = pair_columns(pair), lax.div(tp_peer[pair], 2)
         total = jnp.dot(hcat[...], down_all[:, at], preferred_element_type=jnp.float32)
         rsum[pair // 2] = total.astype(jnp.bfloat16).reshape(tp_n, cap, 2 * width)
         for k in far_first:
             ret_copy[pair, k] = remote(
-                rsum.at[pair // 2, tp_peer[k]], ret.at[t, :, at],
+                rsum.at[pair // 2, tp_peer[k]], ret.at[part, t],
                 ret_s.at[pair // 2, k], ret_r.at[pair // 2, k], f, tp_peer[k],
             )
             ret_copy[pair, k].start()
-        ret[t, :, at] = rsum[pair // 2, t]
+        ret[part, t] = rsum[pair // 2, t]
 
     for k in late[:2]:
         copies[down_m, k].wait_recv()
@@ -406,12 +443,11 @@
     ]
     for copy in copies:
         copy.start()
-    parts = mixed_sems.shape[0]
-    step = mixed.shape[1] // parts
+    parts, _, step = ret_ref.shape
     for i in range(parts):
         at = slice(i * step, (i + 1) * step)
         mixed[:, at] = lax.dot_general(
-            placing_ref[...], ret_ref[:, at], TN, preferred_element_type=jnp.float32
+            placing_ref[...], ret_ref[i], TN, preferred_element_type=jnp.float32
         ).astype(jnp.bfloat16)
         copy = pltpu.make_async_copy(mixed.at[:, at], mixed_out.at[:, at], mixed_sems.at[i])
         copy.start()
@@ -438,7 +474,7 @@
             served,
             served,
             served,
-            jax.ShapeDtypeStruct((tp_n, capacity, model), bf16),
+            jax.ShapeDtypeStruct((tp_n // 2, tp_n, capacity, 2 * width), bf16),
             jax.ShapeDtypeStruct((block, tokens), bf16),
         ),
         in_specs=[hbm] * 7,
@@ -469,6 +505,7 @@
             dma((tp_n,)), dma((tp_n,)),
             dma((fs_n,)), dma((fs_n,)),
             dma((2,)),
+            pltpu.SemaphoreType.REGULAR((2,)),
         ],
         compiler_params=pltpu.CompilerParams(
             collective_id=0, has_side_effects=True, vmem_limit_bytes=44 * 2**20
@@ -492,9 +529,9 @@
         out_shape=(served, served, served, jax.ShapeDtypeStruct((tokens, model), bf16)),
         in_specs=[anywhere, anywhere, anywhere, vmem, vmem],
         out_specs=(hbm,) * 4,
-        scratch_shapes=[pltpu.VMEM((tokens, model), bf16), dma((3,)), dma((4,))],
+        scratch_shapes=[pltpu.VMEM((tokens, model), bf16), dma((3,)), dma((tp_n // 2,))],
         compiler_params=pltpu.CompilerParams(vmem_limit_bytes=16 * 2**20),
-    )(gate_v, up_v, down_v, ret.reshape(block, model), placing)
+    )(gate_v, up_v, down_v, ret.reshape(tp_n // 2, block, 2 * width), placing)
     shape = (1, experts, units, model)
     return gate_serve.reshape(shape), up_serve.reshape(shape), down_serve.reshape(shape), mixed
 

time: 124 us -> 124 us (level)
  no operation moved by 1% of the time
where the time goes in v3:
time: 124 us
  Pallas kernels  123 us (99%)
    pallas_call x1, Pallas kernels, fused_device(): pl.pallas_call(functools.partial(exchange_kernel, dims), out_shape=(serve...  121 us

profile of v3, /device:TPU:0, one launch (start us, length us, event | category | flops | bytes accessed | tf_op | source)
XLA Modules:
  0.0 123.6 jit_solution(1918592958228538584)
XLA Ops:
  0.6 121.1 %shard_map.102 = (bf16[256,2048]{1,0:T(8,128)(2,1)S(1)}, bf16[256,2048]{1,0:T(8,128)(2,1)S(1)}, bf16[256,2048]{1,0:T(8,128)(2,1)S(1)}, bf16[4,8,32,512]{3,2,1,0:T(8,128)(2,1)S(1)}, bf16[256,128]{1,0:T(8,128)(2,1)S(1)}) custom-call(bf16[128,2048]{1,0:T(8,128)(2,1)} %prompt_in.1, f32[1,256]{1,0:T(1,128)} %bitcast.14, f32[8,256,256]{2,1,0:T(8,128)} %bitcast.11, ...), custom_call_target="tpu_custom_call" | custom-call | tf_op jit(solution)/shard_map/pallas_call | solution.py:471
  121.7 1.9 %shard_map.103 = (bf16[256,2048]{1,0:T(8,128)(2,1)}, bf16[256,2048]{1,0:T(8,128)(2,1)}, bf16[256,2048]{1,0:T(8,128)(2,1)}, bf16[128,2048]{1,0:T(8,128)(2,1)}) custom-call(bf16[256,2048]{1,0:T(8,128)(2,1)S(1)} %get-tuple-element.13.gate_in, bf16[256,2048]{1,0:T(8,128)(2,1)S(1)} %get-tuple-element.14.up_in, bf16[256,2048]{1,0:T(8,128)(2,1)S(1)} %get-tuple-element.15.down_in, ...), custom_call_target="tpu_custom_call" | custom-call | tf_op jit(solution)/shard_map/pallas_call | solution.py:527
